TPU v7x, 32 devices: a whole 2x2x4 slice. The times are simulated.
32 devices in a mesh: rep: 2 (over y), fs: 4 (over z), tp: 4 (over x, core).
Axes of the slice: x: 2, y: 2, z: 4, core: 2. Of those that a mesh axis runs over, the one named last changes fastest.
Arguments:
- stream: bfloat16 [4096, 2048], P(('rep', 'fs', 'tp')), may hold values from -6 to 6
- gain_before: float32 [2048], replicated, may hold values from 0.1 to 1.9
- gain_after: float32 [2048], replicated, may hold values from 0.1 to 1.9
- proj_gate: bfloat16 [2048, 3584], P('fs', 'tp'), may hold values from -0.125 to 0.125
- proj_lift: bfloat16 [2048, 3584], P('fs', 'tp'), may hold values from -0.125 to 0.125
- proj_down: bfloat16 [3584, 2048], P('tp', 'fs'), may hold values from -0.09375 to 0.09375
- mixer_gain: float32 [2048], replicated, may hold values from 0.1 to 1.9
- mixer_u: bfloat16 [2048, 2048], P('fs', 'tp'), may hold values from -0.125 to 0.125
- mixer_v: bfloat16 [2048, 2048], P('fs', 'tp'), may hold values from -1 to 1
- layer_gain: float32 [2048], P('tp'), may hold values from 0.1 to 1.9
- layer_shift: float32 [2048], P('tp'), may hold values from -3 to 3
- spatial: bfloat16 [16, 128, 128], P('tp'), may hold values from -0.5 to 0.5
- spatial_shift: float32 [16, 128], P('tp'), may hold values from 0.2 to 2
- mixer_down: bfloat16 [2048, 2048], P('tp', 'fs'), may hold values from -0.125 to 0.125
Outputs:
- result: bfloat16 [4096, 2048], P(('rep', 'fs', 'tp'))
All inputs are finite; a program needn't handle non-finite values.
Results may differ from a plain program's by a relative error of at most 0.017.
Values may be sent and summed in bfloat16 or wider, within the bound.
A program may use at most 128 MiB of HBM per device.

v0:
```python
import jax
import jax.numpy as jnp
from jax import lax
from jax.sharding import PartitionSpec as P

GROUP_DIM = 128
SPAN = 128
A = 2048
norm_epsilon = 1e-06
layer_epsilon = 1e-05


def norm_rows(row_block, scale_gain):
    widened = row_block.astype(jnp.float32)
    factor = lax.rsqrt(jnp.mean(widened * widened, axis=1, keepdims=True) + norm_epsilon)
    return (widened * factor * scale_gain).astype(jnp.bfloat16)


def gathered_norm(stream_rows, scale_gain):
    gathered = lax.all_gather(stream_rows, "tp", axis=0, tiled=True)
    return norm_rows(gathered, scale_gain)


def pair_adder(normed, pieces):
    return (
        jnp.dot(normed, pieces[0], preferred_element_type=jnp.float32),
        jnp.dot(normed, pieces[1], preferred_element_type=jnp.float32),
    )


def activate(gate_vals, lift_vals):
    return (jax.nn.silu(gate_vals) * lift_vals).astype(jnp.bfloat16)


def half_again(stream_rows, scale_gain, proj_gate, proj_lift, proj_down):
    normed = gathered_norm(stream_rows, scale_gain)
    gate_vals, lift_vals = pair_adder(
        normed,
        (
            lax.all_gather(proj_gate, "fs", axis=0, tiled=True),
            lax.all_gather(proj_lift, "fs", axis=0, tiled=True),
        ),
    )
    hidden = activate(gate_vals, lift_vals)
    partial_value = jnp.dot(
        hidden,
        lax.all_gather(proj_down, "fs", axis=1, tiled=True),
        preferred_element_type=jnp.float32,
    )
    summed = lax.psum_scatter(
        partial_value.astype(jnp.bfloat16), "tp", scatter_dimension=0, tiled=True
    ).astype(jnp.float32)
    return (stream_rows.astype(jnp.float32) + 0.5 * summed).astype(jnp.bfloat16)


def token_mixer(
    stream_rows,
    mixer_gain,
    mixer_u,
    mixer_v,
    layer_gain,
    layer_shift,
    spatial,
    spatial_shift,
    mixer_down,
):
    gathered = lax.all_gather(stream_rows, "tp", axis=0, tiled=True)
    normed = norm_rows(gathered, mixer_gain)
    seq_tokens = normed.shape[0]
    u_vals, v_vals = pair_adder(
        normed,
        (
            lax.all_gather(mixer_u, "fs", axis=0, tiled=True),
            lax.all_gather(mixer_v, "fs", axis=0, tiled=True),
        ),
    )
    lifted = jax.nn.gelu(v_vals)
    moments = lax.psum((jnp.sum(lifted, axis=1), jnp.sum(lifted * lifted, axis=1)), "tp")
    centre = moments[0] / A
    spread = moments[1] / A - centre * centre
    normed_v = (
        (lifted - centre[:, None]) * lax.rsqrt(spread[:, None] + layer_epsilon) * layer_gain
        + layer_shift
    ).astype(jnp.bfloat16)
    groups_here = spatial.shape[0]
    blocked = normed_v.reshape(seq_tokens // SPAN, SPAN, groups_here, GROUP_DIM)
    causal = jnp.tril(jnp.ones((SPAN, SPAN), dtype=bool))
    masked = jnp.where(causal[None], spatial, jnp.zeros((), jnp.bfloat16))
    mixed_v = jnp.einsum("gts,bsgd->btgd", masked, blocked, preferred_element_type=jnp.float32)
    mixed_v = mixed_v + spatial_shift.T[None, :, :, None]
    gated = (jax.nn.gelu(u_vals) * mixed_v.reshape(seq_tokens, groups_here * GROUP_DIM)).astype(
        jnp.bfloat16
    )
    partial_value = jnp.dot(
        gated,
        lax.all_gather(mixer_down, "fs", axis=1, tiled=True),
        preferred_element_type=jnp.float32,
    )
    summed = lax.psum_scatter(
        partial_value.astype(jnp.bfloat16), "tp", scatter_dimension=0, tiled=True
    ).astype(jnp.float32)
    return (stream_rows.astype(jnp.float32) + summed).astype(jnp.bfloat16)


def body(
    stream,
    gain_before,
    gain_after,
    proj_gate,
    proj_lift,
    proj_down,
    mixer_gain,
    mixer_u,
    mixer_v,
    layer_gain,
    layer_shift,
    spatial,
    spatial_shift,
    mixer_down,
):
    first = half_again(stream, gain_before, proj_gate, proj_lift, proj_down)
    second = token_mixer(
        first,
        mixer_gain,
        mixer_u,
        mixer_v,
        layer_gain,
        layer_shift,
        spatial,
        spatial_shift,
        mixer_down,
    )
    result = half_again(second, gain_after, proj_gate, proj_lift, proj_down)
    return result


def solution(mesh):
    placed = (
        P(("rep", "fs", "tp"), None),
        P(),
        P(),
        P("fs", "tp"),
        P("fs", "tp"),
        P("tp", "fs"),
        P(),
        P("fs", "tp"),
        P("fs", "tp"),
        P("tp"),
        P("tp"),
        P("tp", None, None),
        P("tp", None),
        P("tp", "fs"),
    )
    return jax.shard_map(
        body, mesh=mesh, in_specs=placed, out_specs=P(("rep", "fs", "tp"), None), check_vma=False
    )
```

profile of v0, /device:TPU:0, one launch (start us, length us, event | category | flops | bytes accessed | tf_op | source)
XLA Modules:
  0.0 575.2 jit_solution(15976335767558670113)
XLA Ops:
  6.5 0.7 all-gather.10.cloned.1.call-update
  7.3 0.0 all-gather.12.cloned.1.call-start
  7.3 0.7 all-gather.12.cloned.1.call-update
  8.0 0.0 all-gather.14.cloned.1.call-start
  8.1 0.7 all-gather.14.cloned.1.call-update
  8.8 0.0 all-gather.16.cloned.1.call-start
  8.8 0.5 all-gather.16.cloned.1.call-update
  9.3 0.0 reduce-scatter.4.cloned.1.call-start
  9.4 24.8 %all-gather.10.cloned.1.call-done = bf16[512,2048]{1,0:T(8,128)(2,1)} async-done(((bf16[128,2048]{1,0:T(8,128)(2,1)}), bf16[512,2048]{1,0:T(8,128)(2,1)}) %all-gather.10.cloned.1.call-update) | async-done | bytes 2097168 | tf_op jit(solution)/shard_map/all_gather | solution.py:20
  34.2 2.2 fusion
  36.4 71.5 %all-gather.12.cloned.1.call-done = bf16[2048,896]{1,0:T(8,128)(2,1)} async-done(((bf16[512,896]{1,0:T(8,128)(2,1)}), bf16[2048,896]{1,0:T(8,128)(2,1)}) %all-gather.12.cloned.1.call-update) | async-done | bytes 3670032 | tf_op jit(solution)/shard_map/all_gather | solution.py:40
  107.9 5.6 fusion.42
  113.5 66.6 %all-gather.14.cloned.1.call-done = bf16[2048,896]{1,0:T(8,128)(2,1)} async-done(((bf16[512,896]{1,0:T(8,128)(2,1)}), bf16[2048,896]{1,0:T(8,128)(2,1)}) %all-gather.14.cloned.1.call-update) | async-done | bytes 3670032 | tf_op jit(solution)/shard_map/all_gather | solution.py:41
  180.2 72.1 %all-gather.16.cloned.1.call-done = bf16[896,2048]{1,0:T(8,128)(2,1)} async-done(((bf16[896,512]{1,0:T(8,128)(2,1)}), bf16[896,2048]{1,0:T(8,128)(2,1)}) %all-gather.16.cloned.1.call-update) | async-done | bytes 3670032 | tf_op jit(solution)/shard_map/all_gather | solution.py:47
  252.3 9.7 %convolution_convert_fusion.1 = bf16[512,2048]{1,0:T(8,128)(2,1)} fusion(bf16[896,2048]{1,0:T(8,128)(2,1)} %all-gather.16.cloned.1.call-done, f32[512,896]{1,0:T(8,128)} %fusion.42, bf16[2048,896]{1,0:T(8,128)(2,1)} %all-gather.14.cloned.1.call-done, bf16[512,2048]{1,0:T(8,128)(2,1)S(1)} %copy-done.4, f32[2048]{0:T(1024)S(1)} %copy-done.10, ...), kind=kOutput, calls=%fused_computation.16 | convolution fusion | flops 3766091776 | bytes 13379584 | tf_op jit(solution)/shard_map/dot_general | solution.py:45
  262.0 0.0 all-gather.18.cloned.1.call-start
  262.0 29.9 %reduce-scatter.4.cloned.1.call-done = bf16[128,2048]{1,0:T(8,128)(2,1)} async-done(((bf16[512,2048]{1,0:T(8,128)(2,1)}), bf16[128,2048]{1,0:T(8,128)(2,1)}) %reduce-scatter.4.cloned.1.call-update) | async-done | bytes 524304 | tf_op jit(solution)/shard_map/reduce_scatter | solution.py:50
  291.9 2.0 add_convert_fusion.3
  293.9 0.0 all-gather.18.cloned.1.call-update
  293.9 0.0 all-gather.22.cloned.1.call-start
  294.0 0.7 all-gather.22.cloned.1.call-update
  294.7 0.0 all-gather.20.cloned.1.call-start
  294.7 0.7 all-gather.20.cloned.1.call-update
  295.4 0.0 all-gather.24.cloned.1.call-start
  295.5 0.7 all-gather.24.cloned.1.call-update
  296.2 0.0 reduce-scatter.6.cloned.1.call-start
  296.2 20.4 %all-gather.18.cloned.1.call-done = bf16[512,2048]{1,0:T(8,128)(2,1)} async-done(((bf16[128,2048]{1,0:T(8,128)(2,1)}), bf16[512,2048]{1,0:T(8,128)(2,1)}) %all-gather.18.cloned.1.call-update) | async-done | bytes 2097168 | tf_op jit(solution)/shard_map/all_gather | solution.py:67
  316.6 2.2 fusion.3
  318.9 45.0 %all-gather.22.cloned.1.call-done = bf16[2048,512]{1,0:T(8,128)(2,1)} async-done(((bf16[512,512]{1,0:T(8,128)(2,1)}), bf16[2048,512]{1,0:T(8,128)(2,1)}) %all-gather.22.cloned.1.call-update) | async-done | bytes 2097168 | tf_op jit(solution)/shard_map/all_gather | solution.py:74
  363.9 4.1 fusion.60
  368.0 6.5 %all-reduce = (f32[512]{0:T(512)S(1)}, f32[512]{0:T(512)S(1)}) all-reduce(f32[512]{0:T(512)S(1)} %get-tuple-element.6, f32[512]{0:T(512)S(1)} %get-tuple-element.5), channel_id=1, replica_groups=mesh['rep'=2,'fs'=4,'tp'=4] {'tp'}, use_global_device_ids=true, to_apply=%region_6.7 | all-reduce | flops 1024 | bytes 8192 | tf_op jit(solution)/shard_map/psum | solution.py:78
  374.6 1.5 add_convert_fusion.2
  376.0 0.9 reshape.47
  377.0 1.4 fusion.9
  378.4 1.3 copy.21
  379.7 30.2 %all-gather.20.cloned.1.call-done = bf16[2048,512]{1,0:T(8,128)(2,1)} async-done(((bf16[512,512]{1,0:T(8,128)(2,1)}), bf16[2048,512]{1,0:T(8,128)(2,1)}) %all-gather.20.cloned.1.call-update) | async-done | bytes 2097168 | tf_op jit(solution)/shard_map/all_gather | solution.py:73
  409.9 46.1 %all-gather.24.cloned.1.call-done = bf16[512,2048]{1,0:T(8,128)(2,1)} async-done(((bf16[512,512]{1,0:T(8,128)(2,1)}), bf16[512,2048]{1,0:T(8,128)(2,1)}) %all-gather.24.cloned.1.call-update) | async-done | bytes 2097168 | tf_op jit(solution)/shard_map/all_gather | solution.py:96
  456.0 6.5 %convolution_convert_fusion.2 = bf16[512,2048]{1,0:T(8,128)(2,1)} fusion(bf16[512,2048]{1,0:T(8,128)(2,1)} %all-gather.24.cloned.1.call-done, f32[64,8,4,128]{3,2,1,0:T(4,128)} %bitcast.25, bf16[2048,512]{1,0:T(8,128)(2,1)} %all-gather.20.cloned.1.call-done, bf16[512,2048]{1,0:T(8,128)(2,1)S(1)} %copy-done.3, f32[2048]{0:T(1024)S(1)} %copy-done.11, ...), kind=kOutput, calls=%fused_computation.17 | convolution fusion | flops 2155347968 | bytes 9447424 | tf_op jit(solution)/shard_map/dot_general | solution.py:94
  462.5 0.0 all-gather.26.cloned.1.call-start
  462.6 30.1 %reduce-scatter.6.cloned.1.call-done = bf16[128,2048]{1,0:T(8,128)(2,1)} async-done(((bf16[512,2048]{1,0:T(8,128)(2,1)}), bf16[128,2048]{1,0:T(8,128)(2,1)}) %reduce-scatter.6.cloned.1.call-update) | async-done | bytes 524304 | tf_op jit(solution)/shard_map/reduce_scatter | solution.py:99
  492.7 2.0 add_convert_fusion.1
  494.6 0.2 reduce-scatter.8.cloned.1.call-start
  494.9 22.5 %all-gather.26.cloned.1.call-done = bf16[512,2048]{1,0:T(8,128)(2,1)} async-done(((bf16[128,2048]{1,0:T(8,128)(2,1)}), bf16[512,2048]{1,0:T(8,128)(2,1)}) %all-gather.26.cloned.1.call-update) | async-done | bytes 2097168 | tf_op jit(solution)/shard_map/all_gather | solution.py:20
  517.4 2.2 fusion.6
  519.6 5.7 fusion.28
  525.3 9.7 %convolution_convert_fusion = bf16[512,2048]{1,0:T(8,128)(2,1)} fusion(bf16[896,2048]{1,0:T(8,128)(2,1)} %all-gather.16.cloned.1.call-done, f32[512,896]{1,0:T(8,128)} %fusion.28, bf16[2048,896]{1,0:T(8,128)(2,1)} %all-gather.14.cloned.1.call-done, bf16[512,2048]{1,0:T(8,128)(2,1)S(1)} %copy-done.5, f32[2048]{0:T(1024)S(1)} %copy-done.12, ...), kind=kOutput, calls=%fused_computation.15 | convolution fusion | flops 3766091776 | bytes 13379584 | tf_op jit(solution)/shard_map/dot_general | solution.py:45
  535.0 31.3 %reduce-scatter.8.cloned.1.call-done = bf16[128,2048]{1,0:T(8,128)(2,1)} async-done(((bf16[512,2048]{1,0:T(8,128)(2,1)}), bf16[128,2048]{1,0:T(8,128)(2,1)}) %reduce-scatter.8.cloned.1.call-update) | async-done | bytes 524304 | tf_op jit(solution)/shard_map/reduce_scatter | solution.py:50
  566.4 2.0 add_convert_fusion
  (36 shorter events, 0.2 us)
Async XLA Ops:
  6.5 27.7 %all-gather.10.cloned.1.call-start = ((), (), s32[]{:S(2)}) async-start(), calls=%async_computation.3 | async-start | bytes 2621440 | tf_op jit(solution)/shard_map/all_gather | solution.py:20
  7.3 100.6 %all-gather.12.cloned.1.call-start = ((), (), s32[]{:S(2)}) async-start(), calls=%async_computation.4 | async-start | bytes 4587520 | tf_op jit(solution)/shard_map/all_gather | solution.py:40
  8.0 99.9 %copy-start.10 = (f32[2048]{0:T(1024)S(1)}, f32[2048]{0:T(1024)}, u32[]{:S(2)}) copy-start(f32[2048]{0:T(1024)} %param.15) | copy-start | bytes 24580
  8.0 172.2 %all-gather.14.cloned.1.call-start = ((), (), s32[]{:S(2)}) async-start(), calls=%async_computation.5 | async-start | bytes 4587520 | tf_op jit(solution)/shard_map/all_gather | solution.py:41
  8.8 243.5 %all-gather.16.cloned.1.call-start = ((), (), s32[]{:S(2)}) async-start(), calls=%async_computation.6 | async-start | bytes 4587520 | tf_op jit(solution)/shard_map/all_gather | solution.py:47
  9.3 282.6 %reduce-scatter.4.cloned.1.call-start = ((), (), s32[]{:S(2)}) async-start(), calls=%async_computation.7 | async-start | bytes 2621440 | tf_op jit(solution)/shard_map/reduce_scatter | solution.py:50
  34.2 73.7 %copy-start.4 = (bf16[512,2048]{1,0:T(8,128)(2,1)S(1)}, bf16[512,2048]{1,0:T(8,128)(2,1)}, u32[]{:S(2)}) copy-start(bf16[512,2048]{1,0:T(8,128)(2,1)} %all-gather.10.cloned.1.call-done) | copy-start | bytes 6291460
  262.0 29.9 %copy-start.2 = (bf16[128,2048]{1,0:T(8,128)(2,1)S(1)}, bf16[128,2048]{1,0:T(8,128)(2,1)}, u32[]{:S(2)}) copy-start(bf16[128,2048]{1,0:T(8,128)(2,1)} %param.14) | copy-start | bytes 1572868
  262.0 54.6 %all-gather.18.cloned.1.call-start = ((), (), s32[]{:S(2)}) async-start(), calls=%async_computation.8 | async-start | bytes 2621440 | tf_op jit(solution)/shard_map/all_gather | solution.py:67
  293.9 70.0 %copy-start.11 = (f32[2048]{0:T(1024)S(1)}, f32[2048]{0:T(1024)}, u32[]{:S(2)}) copy-start(f32[2048]{0:T(1024)} %param.20) | copy-start | bytes 24580
  293.9 70.0 %all-gather.22.cloned.1.call-start = ((), (), s32[]{:S(2)}) async-start(), calls=%async_computation.10 | async-start | bytes 2621440 | tf_op jit(solution)/shard_map/all_gather | solution.py:74
  294.7 115.3 %all-gather.20.cloned.1.call-start = ((), (), s32[]{:S(2)}) async-start(), calls=%async_computation.9 | async-start | bytes 2621440 | tf_op jit(solution)/shard_map/all_gather | solution.py:73
  295.4 160.6 %all-gather.24.cloned.1.call-start = ((), (), s32[]{:S(2)}) async-start(), calls=%async_computation.11 | async-start | bytes 2621440 | tf_op jit(solution)/shard_map/all_gather | solution.py:96
  296.2 196.5 %reduce-scatter.6.cloned.1.call-start = ((), (), s32[]{:S(2)}) async-start(), calls=%async_computation.12 | async-start | bytes 2621440 | tf_op jit(solution)/shard_map/reduce_scatter | solution.py:99
  316.6 47.3 %copy-start.3 = (bf16[512,2048]{1,0:T(8,128)(2,1)S(1)}, bf16[512,2048]{1,0:T(8,128)(2,1)}, u32[]{:S(2)}) copy-start(bf16[512,2048]{1,0:T(8,128)(2,1)} %all-gather.18.cloned.1.call-done) | copy-start | bytes 6291460
  318.9 55.7 %copy-start.7 = (f32[512]{0:T(512)S(1)}, f32[512]{0:T(512)}, u32[]{:S(2)}) copy-start(f32[512]{0:T(512)} %param.24) | copy-start | bytes 6148
  318.9 55.7 %copy-start.8 = (f32[512]{0:T(512)S(1)}, f32[512]{0:T(512)}, u32[]{:S(2)}) copy-start(f32[512]{0:T(512)} %param.23) | copy-start | bytes 6148
  368.0 8.9 %copy-start.6 = (bf16[4,128,128]{2,1,0:T(8,128)(2,1)S(1)}, bf16[4,128,128]{2,1,0:T(8,128)(2,1)}, u32[]{:S(2)}) copy-start(bf16[4,128,128]{2,1,0:T(8,128)(2,1)} %param.25) | copy-start | bytes 393220
  368.0 8.9 %copy-start.9 = (f32[4,128]{1,0:T(4,128)S(1)}, f32[4,128]{1,0:T(4,128)}, u32[]{:S(2)}) copy-start(f32[4,128]{1,0:T(4,128)} %param.26) | copy-start | bytes 6148
  462.5 30.2 %copy-start = (bf16[128,2048]{1,0:T(8,128)(2,1)S(1)}, bf16[128,2048]{1,0:T(8,128)(2,1)}, u32[]{:S(2)}) copy-start(bf16[128,2048]{1,0:T(8,128)(2,1)} %add_convert_fusion.3) | copy-start | bytes 1572868
  462.5 57.1 %copy-start.12 = (f32[2048]{0:T(1024)S(1)}, f32[2048]{0:T(1024)}, u32[]{:S(2)}) copy-start(f32[2048]{0:T(1024)} %param.16) | copy-start | bytes 24580
  462.5 54.8 %all-gather.26.cloned.1.call-start = ((), (), s32[]{:S(2)}) async-start(), calls=%async_computation.13 | async-start | bytes 2621440 | tf_op jit(solution)/shard_map/all_gather | solution.py:20
  494.6 71.7 %reduce-scatter.8.cloned.1.call-start = ((), (), s32[]{:S(2)}) async-start(), calls=%async_computation.14 | async-start | bytes 2621440 | tf_op jit(solution)/shard_map/reduce_scatter | solution.py:50
  517.4 2.2 copy-start.5
  535.0 31.4 %copy-start.1 = (bf16[128,2048]{1,0:T(8,128)(2,1)S(1)}, bf16[128,2048]{1,0:T(8,128)(2,1)}, u32[]{:S(2)}) copy-start(bf16[128,2048]{1,0:T(8,128)(2,1)} %add_convert_fusion.1) | copy-start | bytes 1572868
Sparse Core Ops, SparseCore 0:
  8.9 25.2 all-gather.9
  35.8 72.0 all-gather.11
  109.5 70.6 all-gather.13
  181.6 70.6 all-gather.15
  262.1 29.7 reduce-scatter.3
  294.1 22.5 all-gather.17
  318.2 45.6 all-gather.21
  365.5 44.4 all-gather.19
  411.5 44.4 all-gather.23
  462.6 29.9 reduce-scatter.5
  494.8 22.5 all-gather.25
  535.1 31.1 reduce-scatter.7
where the time goes:
time: 576 us; the launch traced here: 575 us
  waiting for transfers between devices  495 us (86%)
  matrix products  42.7 us (7%)
  other arithmetic  14.1 us (2%)
  between operations  13.7 us (2%)
  blocking collectives  6.51 us (1%)
    all_gather x1, waiting for transfers between devices, half_again(): lax.all_gather(proj_down, 'fs', axis=1, tiled=True)  72.1 us
    all_gather x1, waiting for transfers between devices, half_again(): lax.all_gather(proj_gate, 'fs', axis=0, tiled=True)  71.5 us
    all_gather x1, waiting for transfers between devices, half_again(): lax.all_gather(proj_lift, 'fs', axis=0, tiled=True)  66.6 us
    reduce_scatter x2, waiting for transfers between devices, half_again(): lax.psum_scatter(partial_value.astype(jnp.bfloat16), 'tp', scatter_dimens...  61.2 us
    all_gather x2, waiting for transfers between devices, gathered_norm(): gathered = lax.all_gather(stream_rows, 'tp', axis=0, tiled=True)  47.3 us
    all_gather x1, waiting for transfers between devices, token_mixer(): lax.all_gather(mixer_down, 'fs', axis=1, tiled=True)  46.1 us
    all_gather x1, waiting for transfers between devices, token_mixer(): lax.all_gather(mixer_v, 'fs', axis=0, tiled=True)  45 us
    all_gather x1, waiting for transfers between devices, token_mixer(): lax.all_gather(mixer_u, 'fs', axis=0, tiled=True)  30.2 us
  transfers between devices with their start and end apart: 12, of which 12 were waited for; matrix products, arithmetic and copies ran while one was open for 3% of the time, Pallas kernels for 0%

commit v1 on v0

--- a/solution.py
+++ b/solution.py
@@ -8,6 +8,11 @@
 A = 2048
 norm_epsilon = 1e-06
 layer_epsilon = 1e-05
+
+
+def finish_cube_here(content):
+    earlier = jnp.concatenate(lax.all_gather(content, "fs"), axis=1)
+    return earlier
 
 
 def norm_rows(row_block, scale_gain):
@@ -91,11 +96,7 @@
     gated = (jax.nn.gelu(u_vals) * mixed_v.reshape(seq_tokens, groups_here * GROUP_DIM)).astype(
         jnp.bfloat16
     )
-    partial_value = jnp.dot(
-        gated,
-        lax.all_gather(mixer_down, "fs", axis=1, tiled=True),
-        preferred_element_type=jnp.float32,
-    )
+    partial_value = jnp.dot(gated, finish_cube_here(mixer_down), preferred_element_type=jnp.float32)
     summed = lax.psum_scatter(
         partial_value.astype(jnp.bfloat16), "tp", scatter_dimension=0, tiled=True
     ).astype(jnp.float32)

time: 576 us -> 575 us (level)
  transfers between devices with their start and end apart: 12 -> 12, of which waited for: 12 -> 12; matrix products, arithmetic and copies ran while one was open for 3% -> 4% of each run, Pallas kernels for 0% -> 0%
where the time goes in v1:
time: 575 us; the launch traced here: 574 us
  waiting for transfers between devices  490 us (85%)
  matrix products  42.7 us (7%)
  other arithmetic  14.1 us (2%)
  between operations  13.7 us (2%)
  blocking collectives  6.5 us (1%)
  local copies, waits for them, and re-layouts  6.48 us (1%)
    all_gather x1, waiting for transfers between devices, half_again(): lax.all_gather(proj_down, 'fs', axis=1, tiled=True)  72.1 us
    all_gather x1, waiting for transfers between devices, half_again(): lax.all_gather(proj_gate, 'fs', axis=0, tiled=True)  71.5 us
    all_gather x1, waiting for transfers between devices, half_again(): lax.all_gather(proj_lift, 'fs', axis=0, tiled=True)  66.6 us
    reduce_scatter x2, waiting for transfers between devices, half_again(): lax.psum_scatter(partial_value.astype(jnp.bfloat16), 'tp', scatter_dimens...  60.6 us
    all_gather x2, waiting for transfers between devices, gathered_norm(): gathered = lax.all_gather(stream_rows, 'tp', axis=0, tiled=True)  47.3 us
    all_gather x1, waiting for transfers between devices, token_mixer(): lax.all_gather(mixer_v, 'fs', axis=0, tiled=True)  45 us
    all_gather x1, waiting for transfers between devices, finish_cube_here(): earlier = jnp.concatenate(lax.all_gather(content, 'fs'), axis=1)  43.5 us
    all_gather x1, waiting for transfers between devices, token_mixer(): lax.all_gather(mixer_u, 'fs', axis=0, tiled=True)  30.3 us
  transfers between devices with their start and end apart: 12, of which 12 were waited for; matrix products, arithmetic and copies ran while one was open for 4% of the time, Pallas kernels for 0%

profile of v1, /device:TPU:0, one launch (start us, length us, event | category | flops | bytes accessed | tf_op | source)
XLA Modules:
  0.0 574.4 jit_solution(12445985912097838420)
XLA Ops:
  6.5 0.7 all-gather.11.cloned.1.call-update
  7.3 0.0 all-gather.13.cloned.1.call-start
  7.3 0.7 all-gather.13.cloned.1.call-update
  8.0 0.0 all-gather.15.cloned.1.call-start
  8.1 0.7 all-gather.15.cloned.1.call-update
  8.8 0.0 all-gather.17.cloned.1.call-start
  8.8 0.5 all-gather.17.cloned.1.call-update
  9.3 0.0 reduce-scatter.4.cloned.1.call-start
  9.4 24.8 %all-gather.11.cloned.1.call-done = bf16[512,2048]{1,0:T(8,128)(2,1)} async-done(((bf16[128,2048]{1,0:T(8,128)(2,1)}), bf16[512,2048]{1,0:T(8,128)(2,1)}) %all-gather.11.cloned.1.call-update) | async-done | bytes 2097168 | tf_op jit(solution)/shard_map/all_gather | solution.py:25
  34.2 2.2 fusion
  36.4 71.5 %all-gather.13.cloned.1.call-done = bf16[2048,896]{1,0:T(8,128)(2,1)} async-done(((bf16[512,896]{1,0:T(8,128)(2,1)}), bf16[2048,896]{1,0:T(8,128)(2,1)}) %all-gather.13.cloned.1.call-update) | async-done | bytes 3670032 | tf_op jit(solution)/shard_map/all_gather | solution.py:45
  107.9 5.6 fusion.42
  113.5 66.6 %all-gather.15.cloned.1.call-done = bf16[2048,896]{1,0:T(8,128)(2,1)} async-done(((bf16[512,896]{1,0:T(8,128)(2,1)}), bf16[2048,896]{1,0:T(8,128)(2,1)}) %all-gather.15.cloned.1.call-update) | async-done | bytes 3670032 | tf_op jit(solution)/shard_map/all_gather | solution.py:46
  180.2 72.1 %all-gather.17.cloned.1.call-done = bf16[896,2048]{1,0:T(8,128)(2,1)} async-done(((bf16[896,512]{1,0:T(8,128)(2,1)}), bf16[896,2048]{1,0:T(8,128)(2,1)}) %all-gather.17.cloned.1.call-update) | async-done | bytes 3670032 | tf_op jit(solution)/shard_map/all_gather | solution.py:52
  252.3 9.7 %convolution_convert_fusion.1 = bf16[512,2048]{1,0:T(8,128)(2,1)} fusion(bf16[896,2048]{1,0:T(8,128)(2,1)} %all-gather.17.cloned.1.call-done, f32[512,896]{1,0:T(8,128)} %fusion.42, bf16[2048,896]{1,0:T(8,128)(2,1)} %all-gather.15.cloned.1.call-done, bf16[512,2048]{1,0:T(8,128)(2,1)S(1)} %copy-done.4, f32[2048]{0:T(1024)S(1)} %copy-done.10, ...), kind=kOutput, calls=%fused_computation.16 | convolution fusion | flops 3766091776 | bytes 13379584 | tf_op jit(solution)/shard_map/dot_general | solution.py:50
  262.0 0.0 all-gather.27.cloned.1.call-start
  262.0 0.5 all-gather.27.cloned.1.call-update
  262.6 0.0 all-gather.19.cloned.1.call-start
  262.6 29.3 %reduce-scatter.4.cloned.1.call-done = bf16[128,2048]{1,0:T(8,128)(2,1)} async-done(((bf16[512,2048]{1,0:T(8,128)(2,1)}), bf16[128,2048]{1,0:T(8,128)(2,1)}) %reduce-scatter.4.cloned.1.call-update) | async-done | bytes 524304 | tf_op jit(solution)/shard_map/reduce_scatter | solution.py:55
  291.9 2.0 add_convert_fusion.3
  293.9 0.0 all-gather.23.cloned.1.call-start
  294.0 0.7 all-gather.23.cloned.1.call-update
  294.7 0.0 all-gather.21.cloned.1.call-start
  294.7 0.7 all-gather.21.cloned.1.call-update
  295.4 0.0 reduce-scatter.6.cloned.1.call-start
  295.5 43.5 %all-gather.27.cloned.1.call-done = bf16[2048,512]{1,0:T(8,128)(2,1)} async-done(((bf16[512,512]{1,0:T(8,128)(2,1)}), bf16[2048,512]{1,0:T(8,128)(2,1)}) %all-gather.27.cloned.1.call-update) | async-done | bytes 2097168 | tf_op jit(solution)/shard_map/all_gather | solution.py:14
  339.0 4.1 copy.36
  343.1 18.8 %all-gather.19.cloned.1.call-done = bf16[512,2048]{1,0:T(8,128)(2,1)} async-done(((bf16[128,2048]{1,0:T(8,128)(2,1)}), bf16[512,2048]{1,0:T(8,128)(2,1)}) %all-gather.19.cloned.1.call-update) | async-done | bytes 2097168 | tf_op jit(solution)/shard_map/all_gather | solution.py:72
  362.0 2.2 fusion.3
  364.2 45.0 %all-gather.23.cloned.1.call-done = bf16[2048,512]{1,0:T(8,128)(2,1)} async-done(((bf16[512,512]{1,0:T(8,128)(2,1)}), bf16[2048,512]{1,0:T(8,128)(2,1)}) %all-gather.23.cloned.1.call-update) | async-done | bytes 2097168 | tf_op jit(solution)/shard_map/all_gather | solution.py:79
  409.2 4.1 fusion.60
  413.4 6.5 %all-reduce = (f32[512]{0:T(512)S(1)}, f32[512]{0:T(512)S(1)}) all-reduce(f32[512]{0:T(512)S(1)} %get-tuple-element.6, f32[512]{0:T(512)S(1)} %get-tuple-element.5), channel_id=1, replica_groups=mesh['rep'=2,'fs'=4,'tp'=4] {'tp'}, use_global_device_ids=true, to_apply=%region_6.7 | all-reduce | flops 1024 | bytes 8192 | tf_op jit(solution)/shard_map/psum | solution.py:83
  419.9 1.5 add_convert_fusion.2
  421.4 0.9 reshape.53
  422.3 1.4 fusion.9
  423.7 1.3 copy.35
  425.0 30.3 %all-gather.21.cloned.1.call-done = bf16[2048,512]{1,0:T(8,128)(2,1)} async-done(((bf16[512,512]{1,0:T(8,128)(2,1)}), bf16[2048,512]{1,0:T(8,128)(2,1)}) %all-gather.21.cloned.1.call-update) | async-done | bytes 2097168 | tf_op jit(solution)/shard_map/all_gather | solution.py:78
  455.3 6.5 %convolution_convert_fusion.2 = bf16[512,2048]{1,0:T(8,128)(2,1)} fusion(bf16[512,2048]{0,1:T(8,128)(2,1)} %bitcast.29, f32[64,8,4,128]{3,2,1,0:T(4,128)} %bitcast.31, bf16[2048,512]{1,0:T(8,128)(2,1)} %all-gather.21.cloned.1.call-done, bf16[512,2048]{1,0:T(8,128)(2,1)S(1)} %copy-done.3, f32[2048]{0:T(1024)S(1)} %copy-done.11, f32[512]{0:T(512)S(1)} %add_rsqrt_fusion.2), kind=kOutput, calls=%fused_computation.17 | convolution fusion | flops 2155347968 | bytes 9447424 | tf_op jit(solution)/shard_map/dot_general | solution.py:99
  461.8 0.0 all-gather.25.cloned.1.call-start
  461.8 30.1 %reduce-scatter.6.cloned.1.call-done = bf16[128,2048]{1,0:T(8,128)(2,1)} async-done(((bf16[512,2048]{1,0:T(8,128)(2,1)}), bf16[128,2048]{1,0:T(8,128)(2,1)}) %reduce-scatter.6.cloned.1.call-update) | async-done | bytes 524304 | tf_op jit(solution)/shard_map/reduce_scatter | solution.py:100
  491.9 2.0 add_convert_fusion.1
  493.9 0.2 reduce-scatter.8.cloned.1.call-start
  494.1 22.5 %all-gather.25.cloned.1.call-done = bf16[512,2048]{1,0:T(8,128)(2,1)} async-done(((bf16[128,2048]{1,0:T(8,128)(2,1)}), bf16[512,2048]{1,0:T(8,128)(2,1)}) %all-gather.25.cloned.1.call-update) | async-done | bytes 2097168 | tf_op jit(solution)/shard_map/all_gather | solution.py:25
  516.6 2.2 fusion.6
  518.9 5.7 fusion.28
  524.6 9.7 %convolution_convert_fusion = bf16[512,2048]{1,0:T(8,128)(2,1)} fusion(bf16[896,2048]{1,0:T(8,128)(2,1)} %all-gather.17.cloned.1.call-done, f32[512,896]{1,0:T(8,128)} %fusion.28, bf16[2048,896]{1,0:T(8,128)(2,1)} %all-gather.15.cloned.1.call-done, bf16[512,2048]{1,0:T(8,128)(2,1)S(1)} %copy-done.5, f32[2048]{0:T(1024)S(1)} %copy-done.12, ...), kind=kOutput, calls=%fused_computation.15 | convolution fusion | flops 3766091776 | bytes 13379584 | tf_op jit(solution)/shard_map/dot_general | solution.py:50
  534.3 31.3 %reduce-scatter.8.cloned.1.call-done = bf16[128,2048]{1,0:T(8,128)(2,1)} async-done(((bf16[512,2048]{1,0:T(8,128)(2,1)}), bf16[128,2048]{1,0:T(8,128)(2,1)}) %reduce-scatter.8.cloned.1.call-update) | async-done | bytes 524304 | tf_op jit(solution)/shard_map/reduce_scatter | solution.py:55
  565.6 2.0 add_convert_fusion
  (37 shorter events, 0.2 us)
Async XLA Ops:
  6.5 27.7 %all-gather.11.cloned.1.call-start = ((), (), s32[]{:S(2)}) async-start(), calls=%async_computation.3 | async-start | bytes 2621440 | tf_op jit(solution)/shard_map/all_gather | solution.py:25
  7.3 100.6 %all-gather.13.cloned.1.call-start = ((), (), s32[]{:S(2)}) async-start(), calls=%async_computation.4 | async-start | bytes 4587520 | tf_op jit(solution)/shard_map/all_gather | solution.py:45
  8.0 99.9 %copy-start.10 = (f32[2048]{0:T(1024)S(1)}, f32[2048]{0:T(1024)}, u32[]{:S(2)}) copy-start(f32[2048]{0:T(1024)} %param.15) | copy-start | bytes 24580
  8.0 172.2 %all-gather.15.cloned.1.call-start = ((), (), s32[]{:S(2)}) async-start(), calls=%async_computation.5 | async-start | bytes 4587520 | tf_op jit(solution)/shard_map/all_gather | solution.py:46
  8.8 243.5 %all-gather.17.cloned.1.call-start = ((), (), s32[]{:S(2)}) async-start(), calls=%async_computation.6 | async-start | bytes 4587520 | tf_op jit(solution)/shard_map/all_gather | solution.py:52
  9.3 282.6 %reduce-scatter.4.cloned.1.call-start = ((), (), s32[]{:S(2)}) async-start(), calls=%async_computation.7 | async-start | bytes 2621440 | tf_op jit(solution)/shard_map/reduce_scatter | solution.py:55
  34.2 73.7 %copy-start.4 = (bf16[512,2048]{1,0:T(8,128)(2,1)S(1)}, bf16[512,2048]{1,0:T(8,128)(2,1)}, u32[]{:S(2)}) copy-start(bf16[512,2048]{1,0:T(8,128)(2,1)} %all-gather.11.cloned.1.call-done) | copy-start | bytes 6291460
  262.0 29.9 %copy-start.2 = (bf16[128,2048]{1,0:T(8,128)(2,1)S(1)}, bf16[128,2048]{1,0:T(8,128)(2,1)}, u32[]{:S(2)}) copy-start(bf16[128,2048]{1,0:T(8,128)(2,1)} %param.14) | copy-start | bytes 1572868
  262.0 77.0 %all-gather.27.cloned.1.call-start = ((), (), s32[]{:S(2)}) async-start(), calls=%async_computation.14 | async-start | bytes 2621440 | tf_op jit(solution)/shard_map/all_gather | solution.py:14
  262.6 99.4 %all-gather.19.cloned.1.call-start = ((), (), s32[]{:S(2)}) async-start(), calls=%async_computation.8 | async-start | bytes 2621440 | tf_op jit(solution)/shard_map/all_gather | solution.py:72
  293.9 115.3 %all-gather.23.cloned.1.call-start = ((), (), s32[]{:S(2)}) async-start(), calls=%async_computation.10 | async-start | bytes 2621440 | tf_op jit(solution)/shard_map/all_gather | solution.py:79
  294.7 160.6 %all-gather.21.cloned.1.call-start = ((), (), s32[]{:S(2)}) async-start(), calls=%async_computation.9 | async-start | bytes 2621440 | tf_op jit(solution)/shard_map/all_gather | solution.py:78
  295.4 196.5 %reduce-scatter.6.cloned.1.call-start = ((), (), s32[]{:S(2)}) async-start(), calls=%async_computation.11 | async-start | bytes 2621440 | tf_op jit(solution)/shard_map/reduce_scatter | solution.py:100
  339.0 70.2 %copy-start.11 = (f32[2048]{0:T(1024)S(1)}, f32[2048]{0:T(1024)}, u32[]{:S(2)}) copy-start(f32[2048]{0:T(1024)} %param.20) | copy-start | bytes 24580
  362.0 47.3 %copy-start.3 = (bf16[512,2048]{1,0:T(8,128)(2,1)S(1)}, bf16[512,2048]{1,0:T(8,128)(2,1)}, u32[]{:S(2)}) copy-start(bf16[512,2048]{1,0:T(8,128)(2,1)} %all-gather.19.cloned.1.call-done) | copy-start | bytes 6291460
  364.2 55.7 %copy-start.7 = (f32[512]{0:T(512)S(1)}, f32[512]{0:T(512)}, u32[]{:S(2)}) copy-start(f32[512]{0:T(512)} %param.24) | copy-start | bytes 6148
  364.2 55.7 %copy-start.8 = (f32[512]{0:T(512)S(1)}, f32[512]{0:T(512)}, u32[]{:S(2)}) copy-start(f32[512]{0:T(512)} %param.23) | copy-start | bytes 6148
  413.4 8.9 %copy-start.6 = (bf16[4,128,128]{2,1,0:T(8,128)(2,1)S(1)}, bf16[4,128,128]{2,1,0:T(8,128)(2,1)}, u32[]{:S(2)}) copy-start(bf16[4,128,128]{2,1,0:T(8,128)(2,1)} %param.25) | copy-start | bytes 393220
  413.4 8.9 %copy-start.9 = (f32[4,128]{1,0:T(4,128)S(1)}, f32[4,128]{1,0:T(4,128)}, u32[]{:S(2)}) copy-start(f32[4,128]{1,0:T(4,128)} %param.26) | copy-start | bytes 6148
  461.8 30.2 %copy-start = (bf16[128,2048]{1,0:T(8,128)(2,1)S(1)}, bf16[128,2048]{1,0:T(8,128)(2,1)}, u32[]{:S(2)}) copy-start(bf16[128,2048]{1,0:T(8,128)(2,1)} %add_convert_fusion.3) | copy-start | bytes 1572868
  461.8 57.1 %copy-start.12 = (f32[2048]{0:T(1024)S(1)}, f32[2048]{0:T(1024)}, u32[]{:S(2)}) copy-start(f32[2048]{0:T(1024)} %param.16) | copy-start | bytes 24580
  461.8 54.8 %all-gather.25.cloned.1.call-start = ((), (), s32[]{:S(2)}) async-start(), calls=%async_computation.12 | async-start | bytes 2621440 | tf_op jit(solution)/shard_map/all_gather | solution.py:25
  493.9 71.7 %reduce-scatter.8.cloned.1.call-start = ((), (), s32[]{:S(2)}) async-start(), calls=%async_computation.13 | async-start | bytes 2621440 | tf_op jit(solution)/shard_map/reduce_scatter | solution.py:55
  516.6 2.2 copy-start.5
  534.2 31.4 %copy-start.1 = (bf16[128,2048]{1,0:T(8,128)(2,1)S(1)}, bf16[128,2048]{1,0:T(8,128)(2,1)}, u32[]{:S(2)}) copy-start(bf16[128,2048]{1,0:T(8,128)(2,1)} %add_convert_fusion.1) | copy-start | bytes 1572868
Sparse Core Ops, SparseCore 0:
  8.9 25.2 all-gather.10
  35.8 72.0 all-gather.12
  109.5 70.6 all-gather.14
  181.6 70.6 all-gather.16
  262.1 29.7 reduce-scatter.3
  293.3 45.6 all-gather.26
  340.6 21.3 all-gather.18
  363.5 45.6 all-gather.22
  410.8 44.4 all-gather.20
  461.9 29.9 reduce-scatter.5
  494.0 22.5 all-gather.24
  534.4 31.1 reduce-scatter.7
